TPU v7x, 32 devices: a whole 2x2x4 slice. The times are simulated.
32 devices in a mesh: grp: 2 (over y), kv: 4 (over z), tp: 4 (over x, core).
Axes of the slice: x: 2, y: 2, z: 4, core: 2. Of those that a mesh axis runs over, the one named last changes fastest.
Arguments:
- stream: bfloat16 [16, 4096], P('grp', 'kv'), parts along dimension 0, may hold values from -6 to 6
- attn_gain: bfloat16 [4096], P('kv'), may hold values from 0.099609375 to 1.8984375
- query_weight: bfloat16 [4096, 4096], P('kv', 'tp'), may hold values from -0.09375 to 0.09375
- query_gain: float32 [64], replicated, may hold values from 0.1 to 1.9
- key_cache: bfloat16 [16, 2048, 1024], P('grp', 'kv', 'tp'), parts along dimension 0, may hold values from -200 to 200
- value_cache: bfloat16 [16, 2048, 1024], P('grp', 'kv', 'tp'), parts along dimension 0, may hold values from -6 to 6
- gate_cache: float32 [16, 16, 2048], P('grp', 'tp', 'kv'), parts along dimension 0, may hold values from -2048 to 0, as said below
- output_weight: bfloat16 [4096, 4096], P('tp', 'kv'), may hold values from -0.75 to 0.75
- mixer_gain: bfloat16 [4096], replicated, may hold values from 0.099609375 to 1.8984375
- up_weight: bfloat16 [16384, 4096], P(('kv', 'tp')), may hold values from -0.09375 to 0.09375
- down_weight: bfloat16 [16384, 4096], P(('kv', 'tp')), may hold values from -0.0625 to 0.0625
Outputs:
- result: bfloat16 [16, 4096], P('grp', ('kv', 'tp')), parts along dimension 0
There are 2 independent parts, one for each index of `grp`. A program takes and returns all parts, laid end to end along the dimension named above; an argument that names none is the same for every part. Nothing has to cross between parts.
Inputs may be any that keep to these rules, and one draw needn't show every extreme that they name: `gate_cache`: cumulative log forget gates: along positions each row never rises.
All inputs are finite; a program needn't handle non-finite values.
Results may differ from a plain program's by a relative error of at most 0.007.
The roundings to bfloat16 on the way count: a program that leaves them out, or rounds other values in their place, can miss the bound.
Values may be sent and summed in bfloat16 or wider, within the bound.
No kernel may reach another device: no remote copies, remote signals or barrier semaphores. Data moves between devices by JAX's collectives and lax.ppermute only.
A program may use at most 64 MiB of HBM per device.

v0:
```python
import jax
import jax.numpy as jnp
from jax import lax
from jax.sharding import PartitionSpec as P

HEAD_DIM = 64
EPS = 1e-06


def rms_scale(values):
    return lax.rsqrt(jnp.mean(values * values, axis=-1, keepdims=True) + EPS)


def block_attention(queries, key_block, value_block, gate_block):
    batch_rows, position_index = (key_block.shape[0], key_block.shape[1])
    kv_local = queries.shape[1]
    key_heads = key_block.reshape(batch_rows, position_index, kv_local, HEAD_DIM)
    value_heads = value_block.reshape(batch_rows, position_index, kv_local, HEAD_DIM)
    scores = jnp.einsum("skgd,spkd->skgp", queries, key_heads, preferred_element_type=jnp.float32)
    scores = scores * HEAD_DIM ** (-0.5) - gate_block[:, :, None, :]
    score_top = jnp.max(scores, axis=-1)
    weights_exp = jnp.exp(scores - score_top[..., None])
    totals = jnp.sum(weights_exp, axis=-1)
    weighted = jnp.einsum(
        "skgp,spkd->skgd",
        weights_exp.astype(jnp.bfloat16),
        value_heads,
        preferred_element_type=jnp.float32,
    )
    return (score_top, totals, weighted)


def per_device(
    stream,
    attn_gain,
    query_weight,
    query_gain,
    key_cache,
    value_cache,
    gate_cache,
    output_weight,
    mixer_gain,
    up_weight,
    down_weight,
):
    batch_rows = stream.shape[0]
    scaled = (stream.astype(jnp.float32) * attn_gain.astype(jnp.float32)).astype(jnp.bfloat16)
    partial_value = jnp.dot(scaled, query_weight, preferred_element_type=jnp.float32)
    query_raw = lax.psum(partial_value, "kv")
    kv_local = key_cache.shape[2] // HEAD_DIM
    heads_local = query_raw.shape[1] // HEAD_DIM
    query_heads = query_raw.reshape(batch_rows, heads_local, HEAD_DIM)
    queries = (query_heads * rms_scale(query_heads) * query_gain).astype(jnp.bfloat16)
    queries = queries.reshape(batch_rows, kv_local, heads_local // kv_local, HEAD_DIM)
    score_top, totals, weighted = block_attention(queries, key_cache, value_cache, gate_cache)
    best = lax.pmax(score_top, "kv")
    factor = jnp.exp(score_top - best)
    totals, weighted = lax.psum((factor * totals, factor[..., None] * weighted), "kv")
    attended = (weighted / totals[..., None]).reshape(batch_rows, heads_local * HEAD_DIM)
    attended = attended.astype(jnp.bfloat16)
    projected = jnp.dot(attended, output_weight, preferred_element_type=jnp.float32)
    projected = lax.psum_scatter(projected, "tp", scatter_dimension=1, tiled=True)
    slice_width = projected.shape[1]
    own_slice = lax.dynamic_slice_in_dim(stream, lax.axis_index("tp") * slice_width, slice_width, 1)
    residual = (own_slice.astype(jnp.float32) + projected).astype(jnp.bfloat16)
    full_rows = lax.all_gather(residual, ("kv", "tp"), axis=1, tiled=True).astype(jnp.float32)
    normed = (full_rows * rms_scale(full_rows) * mixer_gain.astype(jnp.float32)).astype(
        jnp.bfloat16
    )
    up_proj = lax.dot_general(
        normed, up_weight, (((1,), (1,)), ((), ())), preferred_element_type=jnp.float32
    )
    squared = jnp.square(jax.nn.relu(up_proj)).astype(jnp.bfloat16)
    partials = jnp.dot(squared, down_weight, preferred_element_type=jnp.float32)
    summed = lax.psum_scatter(partials, ("kv", "tp"), scatter_dimension=1, tiled=True)
    return (residual.astype(jnp.float32) + summed).astype(jnp.bfloat16)


def solution(mesh):
    in_specs = (
        P("grp", "kv"),
        P("kv"),
        P("kv", "tp"),
        P(),
        P("grp", "kv", "tp"),
        P("grp", "kv", "tp"),
        P("grp", "tp", "kv"),
        P("tp", "kv"),
        P(),
        P(("kv", "tp"), None),
        P(("kv", "tp"), None),
    )
    out_specs = P("grp", ("kv", "tp"))
    return jax.shard_map(
        per_device, mesh=mesh, in_specs=in_specs, out_specs=out_specs, check_vma=False
    )
```

profile of v0, /device:TPU:0, one launch (start us, length us, event | category | flops | bytes accessed | tf_op | source)
XLA Modules:
  0.0 189.7 jit_solution(11805961911175229180)
XLA Ops:
  6.5 0.8 convert_element_type.48
  7.4 0.8 copy-done
  8.1 1.1 fusion.19
  9.2 20.8 %psum.21 = f32[8,1024]{1,0:T(8,128)S(1)} all-reduce(f32[8,1024]{1,0:T(8,128)S(1)} %fusion.19), channel_id=1, replica_groups=mesh['grp'=2,'kv'=4,'tp'=4] {'kv'}, use_global_device_ids=true, to_apply=%region_0.0 | all-reduce | flops 8192 | bytes 65536 | tf_op jit(solution)/shard_map/psum | solution.py:49
  30.1 0.1 reshape.45
  30.2 0.1 reduce_sum.27
  30.4 0.1 copy.19
  30.5 4.0 %copy.20 = bf16[8,512,256]{1,2,0:T(8,128)(2,1)} copy(bf16[8,512,256]{2,1,0:T(8,128)(2,1)} %param.15) | data formatting | bytes 4194304 | tf_op args[4]
  34.5 2.1 %fusion.24 = (f32[8,4,4]{2,1,0:T(4,128)S(1)}, f32[8,4,4,512]{3,2,1,0:T(4,128)S(1)}) fusion(f32[8,4,512]{2,1,0:T(4,128)S(1)} %copy-done.1, bf16[8,512,4,64]{1,3,2,0:T(8,128)(2,1)} %bitcast.15, f32[8,4,4,64]{3,2,1,0:T(4,128)S(1)} %reshape.45, f32[64]{0:T(128)S(1)} %copy-done.3, f32[8,4,4]{2,1,0:T(4,128)S(1)} %copy.19), kind=kOutput, calls=%fused_computation.33 | convolution fusion | flops 8609664 | bytes 2458880 | tf_op jit(solution)/shard_map/skgd,spkd->skgp/dot_general | solution.py:19
  36.6 15.5 %pmax.7 = f32[8,4,4]{2,1,0:T(4,128)S(1)} all-reduce(f32[8,4,4]{2,1,0:T(4,128)S(1)} %get-tuple-element.9), channel_id=1, replica_groups=mesh['grp'=2,'kv'=4,'tp'=4] {'kv'}, use_global_device_ids=true, to_apply=%region_3.0 | all-reduce | flops 128 | bytes 1024 | tf_op jit(solution)/shard_map/pmax | solution.py:56
  52.2 0.2 fusion.4
  52.4 3.9 %copy.21 = bf16[8,512,256]{1,2,0:T(8,128)(2,1)} copy(bf16[8,512,256]{2,1,0:T(8,128)(2,1)} %param.16) | data formatting | bytes 4194304 | tf_op args[5]
  56.4 2.3 %convolution_multiply_fusion.1 = f32[8,4,4,64]{3,2,1,0:T(4,128)S(1)} fusion(bf16[8,512,4,64]{1,3,2,0:T(8,128)(2,1)} %bitcast.16, f32[8,4,4,512]{3,2,1,0:T(4,128)S(1)} %get-tuple-element.10, f32[8,4,4]{2,1,0:T(4,128)S(1)} %get-tuple-element.9, f32[8,4,4]{2,1,0:T(4,128)S(1)} %bitcast.22), kind=kOutput, calls=%fused_computation.2 | convolution fusion | flops 8527872 | bytes 2393088 | tf_op jit(solution)/shard_map/skgp,spkd->skgd/dot_general | solution.py:24
  58.7 17.6 %all-reduce = (f32[8,4,4,64]{3,2,1,0:T(4,128)S(1)}, f32[8,4,4]{2,1,0:T(4,128)S(1)}) all-reduce(f32[8,4,4,64]{3,2,1,0:T(4,128)S(1)} %convolution_multiply_fusion.1, f32[8,4,4]{2,1,0:T(4,128)S(1)} %bitcast.18), channel_id=1, replica_groups=mesh['grp'=2,'kv'=4,'tp'=4] {'kv'}, use_global_device_ids=true, to_apply=%region_4.0 | all-reduce | flops 8320 | bytes 66560 | tf_op jit(solution)/shard_map/psum | solution.py:58
  76.3 0.1 divide_convert_fusion
  76.4 0.1 convert_element_type.53
  76.5 2.6 %fusion.25 = f32[8,1024]{1,0:T(8,128)} fusion(bf16[8,1024]{1,0:T(8,128)(2,1)S(1)} %convert_element_type.53, bf16[1024,1024]{1,0:T(8,128)(2,1)} %param.18), kind=kOutput, calls=%fused_computation.34 | convolution fusion | flops 16777216 | bytes 2146304 | tf_op jit(solution)/shard_map/dot_general | solution.py:61
  79.2 18.2 %reduce-scatter.3.cloned.1.call-done = f32[8,256]{1,0:T(8,128)} async-done(((f32[8,1024]{1,0:T(8,128)}), f32[8,256]{1,0:T(8,128)}) %reduce-scatter.3.cloned.1.call-update) | async-done | bytes 8208 | tf_op jit(solution)/shard_map/reduce_scatter | solution.py:62
  97.4 0.7 add_convert_fusion.1
  98.1 20.6 %all_gather.3 = bf16[8,4096]{1,0:T(8,128)(2,1)S(1)} all-gather(bf16[8,256]{1,0:T(8,128)(2,1)S(1)} %add_convert_fusion.1), channel_id=1, replica_groups=mesh['grp'=2,'kv'=4,'tp'=4] {'kv','tp'}, dimensions={1}, use_global_device_ids=true | all-gather | bytes 69632 | tf_op jit(solution)/shard_map/all_gather | solution.py:66
  118.7 0.1 fusion.6
  118.8 9.8 %fusion.3 = f32[8,4096]{1,0:T(8,128)} fusion(bf16[1024,4096]{1,0:T(8,128)(2,1)} %param.21, bf16[1024,4096]{1,0:T(8,128)(2,1)} %param.20, bf16[8,4096]{1,0:T(8,128)(2,1)S(1)} %all_gather.3, f32[4096]{0:T(1024)S(1)} %convert_element_type.57, f32[8]{0:T(128)S(1)} %add_rsqrt_fusion.1), kind=kOutput, calls=%fused_computation.6 | convolution fusion | flops 134373376 | bytes 16990240 | tf_op jit(solution)/shard_map/dot_general | solution.py:74
  128.6 53.0 %reduce-scatter.5.cloned.1.call-done = f32[8,256]{1,0:T(8,128)} async-done(((f32[8,4096]{1,0:T(8,128)}), f32[8,256]{1,0:T(8,128)}) %reduce-scatter.5.cloned.1.call-update) | async-done | bytes 8208 | tf_op jit(solution)/shard_map/reduce_scatter | solution.py:75
  181.6 1.3 add_convert_fusion
  (18 shorter events, 0.3 us)
Async XLA Ops:
  6.5 1.6 copy-start
  6.5 90.9 %reduce-scatter.3.cloned.1.call-start = ((), (), s32[]{:S(2)}) async-start(), calls=%async_computation.2 | async-start | bytes 40960 | tf_op jit(solution)/shard_map/reduce_scatter | solution.py:62
  30.5 4.0 %copy-start.1 = (f32[8,4,512]{2,1,0:T(4,128)S(1)}, f32[8,4,512]{2,1,0:T(4,128)}, u32[]{:S(2)}) copy-start(f32[8,4,512]{2,1,0:T(4,128)} %param.17) | copy-start | bytes 196612
  30.5 4.0 %copy-start.3 = (f32[64]{0:T(128)S(1)}, f32[64]{0:T(128)}, u32[]{:S(2)}) copy-start(f32[64]{0:T(128)} %param.14) | copy-start | bytes 772
  56.4 22.8 %copy-start.2 = (bf16[4096]{0:T(1024)(128)(2,1)S(1)}, bf16[4096]{0:T(1024)(128)(2,1)}, u32[]{:S(2)}) copy-start(bf16[4096]{0:T(1024)(128)(2,1)} %param.19) | copy-start | bytes 24580
  79.1 102.5 %reduce-scatter.5.cloned.1.call-start = ((), (), s32[]{:S(2)}) async-start(), calls=%async_computation.3 | async-start | bytes 139264 | tf_op jit(solution)/shard_map/reduce_scatter | solution.py:75
Sparse Core Ops, SparseCore 0:
  79.2 18.1 reduce-scatter.2
  128.8 52.8 reduce-scatter.4
where the time goes:
time: 190 us
  blocking collectives  74.5 us (39%)
  waiting for transfers between devices  71.2 us (37%)
  matrix products  17.9 us (9%)
  between operations  13.5 us (7%)
  local copies, waits for them, and re-layouts  9.15 us (5%)
  other arithmetic  3.46 us (2%)
    reduce_scatter x1, waiting for transfers between devices, per_device(): lax.psum_scatter(partials, ('kv', 'tp'), scatter_dimension=1, tiled=True)  53 us
    psum x1, blocking collectives, per_device(): query_raw = lax.psum(partial_value, 'kv')  20.8 us
    all_gather x1, blocking collectives, per_device(): lax.all_gather(residual, ('kv', 'tp'), axis=1, tiled=True)  20.6 us
    reduce_scatter x1, waiting for transfers between devices, per_device(): lax.psum_scatter(projected, 'tp', scatter_dimension=1, tiled=True)  18.2 us
    psum x1, blocking collectives, per_device(): lax.psum((factor * totals, factor[..., None] * weighted), 'kv')  17.6 us
    pmax x1, blocking collectives, per_device(): best = lax.pmax(score_top, 'kv')  15.5 us
    dot_general x1, matrix products, per_device(): partials = jnp.dot(squared, down_weight, preferred_element_type=jnp.float32)  9.78 us
    unnamed x10, local copies, waits for them, and re-layouts  8.7 us
  transfers between devices with their start and end apart: 2, of which 2 were waited for; matrix products, arithmetic and copies ran while one was open for 0% of the time, Pallas kernels for 0%

commit v1 on v0

--- a/solution.py
+++ b/solution.py
@@ -46,7 +46,11 @@
     batch_rows = stream.shape[0]
     scaled = (stream.astype(jnp.float32) * attn_gain.astype(jnp.float32)).astype(jnp.bfloat16)
     partial_value = jnp.dot(scaled, query_weight, preferred_element_type=jnp.float32)
-    query_raw = lax.psum(partial_value, "kv")
+    size = lax.axis_size("kv")
+    query_raw, far = (partial_value, 1)
+    while far < size:
+        query_raw = query_raw + lax.ppermute(query_raw, "kv", [(i, i ^ far) for i in range(size)])
+        far = 2 * far
     kv_local = key_cache.shape[2] // HEAD_DIM
     heads_local = query_raw.shape[1] // HEAD_DIM
     query_heads = query_raw.reshape(batch_rows, heads_local, HEAD_DIM)

time: 190 us -> 179 us (0.942)
  blocking collectives: 74.5 us -> 54.6 us
  starting transfers between devices: 0.04 us -> 6.13 us
  waiting for transfers between devices: 71.2 us -> 73.7 us
    psum x1 -> x0, blocking collectives: 20.8 us -> none  [per_device(): query_raw = lax.psum(partial_value, 'kv')]
    ppermute x0 -> x2, starting transfers between devices: none -> 6.09 us  [per_device(): lax.ppermute(query_raw, 'kv', [(i, i ^ far) for i in range(size)])]
  transfers between devices with their start and end apart: 2 -> 4, of which waited for: 2 -> 3; matrix products, arithmetic and copies ran while one was open for 0% -> 4% of each run, Pallas kernels for 0% -> 0%
where the time goes in v1:
time: 179 us; the launch traced here: 178 us
  waiting for transfers between devices  73.7 us (41%)
  blocking collectives  54.6 us (31%)
  matrix products  17.9 us (10%)
  between operations  13.5 us (8%)
  local copies, waits for them, and re-layouts  9.14 us (5%)
  starting transfers between devices  6.13 us (3%)
  other arithmetic  3.47 us (2%)
    reduce_scatter x1, waiting for transfers between devices, per_device(): lax.psum_scatter(partials, ('kv', 'tp'), scatter_dimension=1, tiled=True)  53 us
    all_gather x1, blocking collectives, per_device(): lax.all_gather(residual, ('kv', 'tp'), axis=1, tiled=True)  20.6 us
    reduce_scatter x1, waiting for transfers between devices, per_device(): lax.psum_scatter(projected, 'tp', scatter_dimension=1, tiled=True)  18.8 us
    psum x1, blocking collectives, per_device(): lax.psum((factor * totals, factor[..., None] * weighted), 'kv')  17 us
    pmax x1, blocking collectives, per_device(): best = lax.pmax(score_top, 'kv')  17 us
    dot_general x1, matrix products, per_device(): partials = jnp.dot(squared, down_weight, preferred_element_type=jnp.float32)  9.78 us
    unnamed x10, local copies, waits for them, and re-layouts  8.7 us
    ppermute x2, starting transfers between devices, per_device(): lax.ppermute(query_raw, 'kv', [(i, i ^ far) for i in range(size)])  6.09 us
  transfers between devices with their start and end apart: 4, of which 3 were waited for; matrix products, arithmetic and copies ran while one was open for 4% of the time, Pallas kernels for 0%

profile of v1, /device:TPU:0, one launch (start us, length us, event | category | flops | bytes accessed | tf_op | source)
XLA Modules:
  0.0 178.4 jit_solution(12828232073183710899)
XLA Ops:
  6.5 0.8 convert_element_type.48
  7.4 0.8 copy-done
  8.1 1.1 fusion.19
  9.2 3.1 %collective-permute-start = (f32[8,1024]{1,0:T(8,128)S(1)}, f32[8,1024]{1,0:T(8,128)S(1)}, u32[]{:S(2)}, u32[]{:S(2)}) collective-permute-start(f32[8,1024]{1,0:T(8,128)S(1)} %fusion.19), channel_id=1, source_target_pairs={{0,4},{4,0},{8,12},{12,8},{1,5},{5,1},{9,13},{13,9},{2,6},{6,2},{1... | collective-permute-start | bytes 98312 | tf_op jit(solution)/shard_map/ppermute | solution.py:52
  12.3 1.9 %collective-permute-done = f32[8,1024]{1,0:T(8,128)S(1)} collective-permute-done((f32[8,1024]{1,0:T(8,128)S(1)}, f32[8,1024]{1,0:T(8,128)S(1)}, u32[]{:S(2)}, u32[]{:S(2)}) %collective-permute-start) | collective-permute-done | bytes 32800 | tf_op jit(solution)/shard_map/ppermute | solution.py:52
  14.2 3.0 %collective-permute-start.1 = (f32[8,1024]{1,0:T(8,128)S(1)}, f32[8,1024]{1,0:T(8,128)S(1)}, u32[]{:S(2)}, u32[]{:S(2)}) collective-permute-start(f32[8,1024]{1,0:T(8,128)S(1)} %add.44), channel_id=1, source_target_pairs={{0,8},{4,12},{8,0},{12,4},{1,9},{5,13},{9,1},{13,5},{2,10},{6,14},... | collective-permute-start | bytes 98312 | tf_op jit(solution)/shard_map/ppermute | solution.py:52
  17.2 3.9 %copy.20 = bf16[8,512,256]{1,2,0:T(8,128)(2,1)} copy(bf16[8,512,256]{2,1,0:T(8,128)(2,1)} %param.15) | data formatting | bytes 4194304 | tf_op args[4]
  21.2 4.0 %copy.21 = bf16[8,512,256]{1,2,0:T(8,128)(2,1)} copy(bf16[8,512,256]{2,1,0:T(8,128)(2,1)} %param.16) | data formatting | bytes 4194304 | tf_op args[5]
  25.4 0.1 copy.19
  25.6 2.1 %fusion.25 = (f32[8,4,4]{2,1,0:T(4,128)S(1)}, f32[8,4,4,512]{3,2,1,0:T(4,128)S(1)}) fusion(f32[8,4,512]{2,1,0:T(4,128)S(1)} %copy-done.1, bf16[8,512,4,64]{1,3,2,0:T(8,128)(2,1)} %bitcast.15, f32[8,4,4,64]{3,2,1,0:T(4,128)S(1)} %reshape.45, f32[64]{0:T(128)S(1)} %copy-done.3, f32[8,4,4]{2,1,0:T(4,128)S(1)} %copy.19), kind=kOutput, calls=%fused_computation.34 | convolution fusion | flops 8609664 | bytes 2458880 | tf_op jit(solution)/shard_map/skgd,spkd->skgp/dot_general | solution.py:19
  27.8 17.0 %pmax.7 = f32[8,4,4]{2,1,0:T(4,128)S(1)} all-reduce(f32[8,4,4]{2,1,0:T(4,128)S(1)} %get-tuple-element.11), channel_id=1, replica_groups=mesh['grp'=2,'kv'=4,'tp'=4] {'kv'}, use_global_device_ids=true, to_apply=%region_2.0 | all-reduce | flops 128 | bytes 1024 | tf_op jit(solution)/shard_map/pmax | solution.py:60
  44.7 0.2 fusion.4
  45.0 2.3 %convolution_multiply_fusion.1 = f32[8,4,4,64]{3,2,1,0:T(4,128)S(1)} fusion(bf16[8,512,4,64]{1,3,2,0:T(8,128)(2,1)} %bitcast.16, f32[8,4,4,512]{3,2,1,0:T(4,128)S(1)} %get-tuple-element.12, f32[8,4,4]{2,1,0:T(4,128)S(1)} %get-tuple-element.11, f32[8,4,4]{2,1,0:T(4,128)S(1)} %bitcast.22), kind=kOutput, calls=%fused_computation.2 | convolution fusion | flops 8527872 | bytes 2393088 | tf_op jit(solution)/shard_map/skgp,spkd->skgd/dot_general | solution.py:24
  47.3 17.0 %all-reduce = (f32[8,4,4,64]{3,2,1,0:T(4,128)S(1)}, f32[8,4,4]{2,1,0:T(4,128)S(1)}) all-reduce(f32[8,4,4,64]{3,2,1,0:T(4,128)S(1)} %convolution_multiply_fusion.1, f32[8,4,4]{2,1,0:T(4,128)S(1)} %bitcast.18), channel_id=1, replica_groups=mesh['grp'=2,'kv'=4,'tp'=4] {'kv'}, use_global_device_ids=true, to_apply=%region_3.0 | all-reduce | flops 8320 | bytes 66560 | tf_op jit(solution)/shard_map/psum | solution.py:62
  64.4 0.1 divide_convert_fusion
  64.5 0.1 convert_element_type.53
  64.6 2.6 %fusion.26 = f32[8,1024]{1,0:T(8,128)} fusion(bf16[8,1024]{1,0:T(8,128)(2,1)S(1)} %convert_element_type.53, bf16[1024,1024]{1,0:T(8,128)(2,1)} %param.18), kind=kOutput, calls=%fused_computation.35 | convolution fusion | flops 16777216 | bytes 2146304 | tf_op jit(solution)/shard_map/dot_general | solution.py:65
  67.2 18.8 %reduce-scatter.3.cloned.1.call-done = f32[8,256]{1,0:T(8,128)} async-done(((f32[8,1024]{1,0:T(8,128)}), f32[8,256]{1,0:T(8,128)}) %reduce-scatter.3.cloned.1.call-update) | async-done | bytes 8208 | tf_op jit(solution)/shard_map/reduce_scatter | solution.py:66
  86.0 0.7 add_convert_fusion.1
  86.7 20.6 %all_gather.3 = bf16[8,4096]{1,0:T(8,128)(2,1)S(1)} all-gather(bf16[8,256]{1,0:T(8,128)(2,1)S(1)} %add_convert_fusion.1), channel_id=1, replica_groups=mesh['grp'=2,'kv'=4,'tp'=4] {'kv','tp'}, dimensions={1}, use_global_device_ids=true | all-gather | bytes 69632 | tf_op jit(solution)/shard_map/all_gather | solution.py:70
  107.3 0.1 fusion.6
  107.5 9.8 %fusion.3 = f32[8,4096]{1,0:T(8,128)} fusion(bf16[1024,4096]{1,0:T(8,128)(2,1)} %param.21, bf16[1024,4096]{1,0:T(8,128)(2,1)} %param.20, bf16[8,4096]{1,0:T(8,128)(2,1)S(1)} %all_gather.3, f32[4096]{0:T(1024)S(1)} %convert_element_type.57, f32[8]{0:T(128)S(1)} %add_rsqrt_fusion.1), kind=kOutput, calls=%fused_computation.6 | convolution fusion | flops 134373376 | bytes 16990240 | tf_op jit(solution)/shard_map/dot_general | solution.py:78
  117.3 53.0 %reduce-scatter.5.cloned.1.call-done = f32[8,256]{1,0:T(8,128)} async-done(((f32[8,4096]{1,0:T(8,128)}), f32[8,256]{1,0:T(8,128)}) %reduce-scatter.5.cloned.1.call-update) | async-done | bytes 8208 | tf_op jit(solution)/shard_map/reduce_scatter | solution.py:79
  170.2 1.3 add_convert_fusion
  (22 shorter events, 0.5 us)
Async XLA Ops:
  6.5 1.6 copy-start
  6.5 79.5 %reduce-scatter.3.cloned.1.call-start = ((), (), s32[]{:S(2)}) async-start(), calls=%async_computation.2 | async-start | bytes 40960 | tf_op jit(solution)/shard_map/reduce_scatter | solution.py:66
  9.2 4.9 %collective-permute-start = (f32[8,1024]{1,0:T(8,128)S(1)}, f32[8,1024]{1,0:T(8,128)S(1)}, u32[]{:S(2)}, u32[]{:S(2)}) collective-permute-start(f32[8,1024]{1,0:T(8,128)S(1)} %fusion.19), channel_id=1, source_target_pairs={{0,4},{4,0},{8,12},{12,8},{1,5},{5,1},{9,13},{13,9},{2,6},{6,2},{1... | collective-permute-start | bytes 98312 | tf_op jit(solution)/shard_map/ppermute | solution.py:52
  14.2 11.0 %collective-permute-start.1 = (f32[8,1024]{1,0:T(8,128)S(1)}, f32[8,1024]{1,0:T(8,128)S(1)}, u32[]{:S(2)}, u32[]{:S(2)}) collective-permute-start(f32[8,1024]{1,0:T(8,128)S(1)} %add.44), channel_id=1, source_target_pairs={{0,8},{4,12},{8,0},{12,4},{1,9},{5,13},{9,1},{13,5},{2,10},{6,14},... | collective-permute-start | bytes 98312 | tf_op jit(solution)/shard_map/ppermute | solution.py:52
  21.2 4.5 %copy-start.1 = (f32[8,4,512]{2,1,0:T(4,128)S(1)}, f32[8,4,512]{2,1,0:T(4,128)}, u32[]{:S(2)}) copy-start(f32[8,4,512]{2,1,0:T(4,128)} %param.17) | copy-start | bytes 196612
  21.2 4.5 %copy-start.3 = (f32[64]{0:T(128)S(1)}, f32[64]{0:T(128)}, u32[]{:S(2)}) copy-start(f32[64]{0:T(128)} %param.14) | copy-start | bytes 772
  45.0 22.2 %copy-start.2 = (bf16[4096]{0:T(1024)(128)(2,1)S(1)}, bf16[4096]{0:T(1024)(128)(2,1)}, u32[]{:S(2)}) copy-start(bf16[4096]{0:T(1024)(128)(2,1)} %param.19) | copy-start | bytes 24580
  67.2 103.1 %reduce-scatter.5.cloned.1.call-start = ((), (), s32[]{:S(2)}) async-start(), calls=%async_computation.3 | async-start | bytes 139264 | tf_op jit(solution)/shard_map/reduce_scatter | solution.py:79
Sparse Core Ops, SparseCore 0:
  67.3 18.6 reduce-scatter.2
  117.4 52.8 reduce-scatter.4
